TPU v7x, 32 devices: a whole 2x2x4 slice. The times are simulated.
32 devices in a mesh: sp: 8 (over z, core), tp: 4 (over y, x).
Axes of the slice: x: 2, y: 2, z: 4, core: 2. Of those that a mesh axis runs over, the one named last changes fastest.
Arguments:
- residual: bfloat16 [896, 2048], P('sp'), may hold values from -1.5 to 1.5
- latent: bfloat16 [896, 512], P('sp'), may hold values from -6 to 6
- rot_key: bfloat16 [896, 64], P('sp'), may hold values from -6 to 6
- latent_norm_scale: float32 [512], replicated, may hold values from 0.1 to 1.9
- query_wide: bfloat16 [896, 3072], P('sp', 'tp'), may hold values from -210 to 210
- query_narrow: bfloat16 [896, 2048], P('sp', 'tp'), may hold values from -210 to 210
- large_key_lift: bfloat16 [512, 2048], P(None, 'tp'), may hold values from -0.25 to 0.25
- large_value_lift: bfloat16 [512, 2048], P(None, 'tp'), may hold values from -0.25 to 0.25
- small_key_lift: bfloat16 [512, 1024], P(None, 'tp'), may hold values from -0.25 to 0.25
- small_value_lift: bfloat16 [512, 1024], P(None, 'tp'), may hold values from -0.25 to 0.25
- out_wide: bfloat16 [2048, 2048], P('tp'), may hold values from -0.5 to 0.5
- out_narrow: bfloat16 [1024, 2048], P('tp'), may hold values from -0.75 to 0.75
- mix_gain: float32 [2048], replicated, may hold values from 0.1 to 1.9
- router_group: bfloat16 [2048, 4], replicated, may hold values from -0.125 to 0.125
- router_expert: bfloat16 [2048, 8], replicated, may hold values from -0.125 to 0.125
- expert_ids: int32 [896, 2], P('sp'), may hold values from 0 to 7, all different within a row; in each aligned block of 112 rows (0 to 111, 112 to 223, ...) at most 56 rows name the same one
- expert_gate_w: bfloat16 [8, 2048, 4096], P('sp', None, 'tp'), may hold values from -0.125 to 0.125
- expert_up_w: bfloat16 [8, 2048, 4096], P('sp', None, 'tp'), may hold values from -0.125 to 0.125
- expert_down_w: bfloat16 [8, 4096, 2048], P('sp', 'tp'), may hold values from -0.375 to 0.375
Outputs:
- updated: bfloat16 [896, 2048], P('sp', 'tp')
Inputs may be any that keep to these rules, and one draw needn't show every extreme that they name: `expert_ids`: each row names two different experts; the rows of one index of sp name no expert more than 56 times, a bound that some expert reaches in some of these blocks.
All inputs are finite; a program needn't handle non-finite values.
Results may differ from a plain program's by a relative error of at most 0.024.
The roundings to bfloat16 on the way count: a program that leaves them out, or rounds other values in their place, can miss the bound.
Values may be sent and summed in bfloat16 or wider, within the bound.
A program may use at most 64 MiB of HBM per device.

v0:
```python
import jax
import jax.numpy as jnp
from jax import lax
from jax.sharding import PartitionSpec as P

PLAIN_KEY_WIDTH = 128
LARGE_VALUE_SIZE = 128
SMALL_HEAD_WIDTH = 64
ROPE = 64
rope_base = 10000.0
epsilon = 1e-06
very_low = -1e30


def angle_table(positions, width):
    frequency = rope_base ** (-jnp.arange(0, width, 2, dtype=jnp.float32) / width)
    return positions.astype(jnp.float32)[:, None] * frequency[None, :]


def rotate(values, angles):
    half_width = values.shape[-1] // 2
    cosine = jnp.cos(angles)
    sine_part = jnp.sin(angles)
    front_half = values[..., :half_width]
    back_half = values[..., half_width:]
    return jnp.concatenate(
        [front_half * cosine - back_half * sine_part, front_half * sine_part + back_half * cosine],
        axis=-1,
    )


def rms_scale(values, gain):
    return values * lax.rsqrt(jnp.mean(values * values, axis=-1, keepdims=True) + epsilon) * gain


def roped_queries(query, plain_width, angles):
    row_count = query.shape[0]
    shaped = query.reshape(row_count, -1, plain_width + ROPE)
    turned = rotate(shaped[..., plain_width:].astype(jnp.float32), angles[:, None, :]).astype(
        jnp.bfloat16
    )
    return jnp.concatenate([shaped[..., :plain_width], turned], axis=-1)


def expand_keys(latent_rows, large_key_lift, large_value_lift, small_key_lift, small_value_lift):
    row_count = latent_rows.shape[0]

    def project(weight, head_width):
        product = jnp.dot(latent_rows, weight, preferred_element_type=jnp.float32).astype(
            jnp.bfloat16
        )
        return product.reshape(row_count, weight.shape[1] // head_width, head_width)

    return (
        project(large_key_lift, PLAIN_KEY_WIDTH),
        project(large_value_lift, LARGE_VALUE_SIZE),
        project(small_key_lift, SMALL_HEAD_WIDTH),
        project(small_value_lift, SMALL_HEAD_WIDTH),
    )


def attend_group(state, queries, plain_width, key_rows, values, key_rot, causal_mask):
    row_peak, weight_sum, summed = state
    score_scale = (plain_width + ROPE) ** (-0.5)
    scores = jnp.einsum(
        "qhd,khd->qhk", queries[..., :plain_width], key_rows, preferred_element_type=jnp.float32
    )
    scores = scores + jnp.einsum(
        "qhd,kd->qhk", queries[..., plain_width:], key_rot, preferred_element_type=jnp.float32
    )
    scores = scores * score_scale
    allowed = causal_mask[:, None, :]
    new_peak = jnp.maximum(row_peak, jnp.max(jnp.where(allowed, scores, very_low), axis=-1))
    weights = jnp.where(allowed, jnp.exp(scores - new_peak[..., None]), 0.0)
    weight_sum = jnp.sum(weights, axis=-1)
    summed = jnp.einsum(
        "qhk,khd->qhd", weights.astype(jnp.bfloat16), values, preferred_element_type=jnp.float32
    )
    return (new_peak, weight_sum, summed)


def shards(
    residual,
    latent,
    rot_key,
    latent_norm_scale,
    query_wide,
    query_narrow,
    large_key_lift,
    large_value_lift,
    small_key_lift,
    small_value_lift,
    out_wide,
    out_narrow,
    mix_gain,
    router_group,
    router_expert,
    expert_ids,
    expert_gate_w,
    expert_up_w,
    expert_down_w,
):
    tok_rows = latent.shape[0]
    positions = lax.axis_index("sp") * tok_rows + jnp.arange(tok_rows, dtype=jnp.int32)
    angles = angle_table(positions, ROPE)
    normed = rms_scale(latent.astype(jnp.float32), latent_norm_scale).astype(jnp.bfloat16)
    key_turned = rotate(rot_key.astype(jnp.float32), angles).astype(jnp.bfloat16)
    wide_queries = roped_queries(query_wide, PLAIN_KEY_WIDTH, angles)
    narrow_queries = roped_queries(query_narrow, SMALL_HEAD_WIDTH, angles)

    def empty_state(head_count, head_width):
        return (
            jnp.full((tok_rows, head_count), very_low, jnp.float32),
            jnp.zeros((tok_rows, head_count), jnp.float32),
            jnp.zeros((tok_rows, head_count, head_width), jnp.float32),
        )

    initial = (
        empty_state(wide_queries.shape[1], LARGE_VALUE_SIZE),
        empty_state(narrow_queries.shape[1], SMALL_HEAD_WIDTH),
    )
    key_set = expand_keys(
        lax.all_gather(normed, "sp", axis=0, tiled=True),
        large_key_lift,
        large_value_lift,
        small_key_lift,
        small_value_lift,
    )
    key_rot = lax.all_gather(key_turned, "sp", axis=0, tiled=True)
    key_positions = jnp.arange(key_rot.shape[0], dtype=jnp.int32)
    causal_mask = positions[:, None] >= key_positions[None, :]
    wide_state = attend_group(
        initial[0], wide_queries, PLAIN_KEY_WIDTH, key_set[0], key_set[1], key_rot, causal_mask
    )
    narrow_state = attend_group(
        initial[1], narrow_queries, SMALL_HEAD_WIDTH, key_set[2], key_set[3], key_rot, causal_mask
    )

    def heads_out(state):
        return (state[2] / state[1][..., None]).astype(jnp.bfloat16).reshape(tok_rows, -1)

    partial_value = jnp.dot(heads_out(wide_state), out_wide, preferred_element_type=jnp.float32)
    partial_value = partial_value + jnp.dot(
        heads_out(narrow_state), out_narrow, preferred_element_type=jnp.float32
    )
    rounded_partial = lax.optimization_barrier(partial_value.astype(jnp.bfloat16)).astype(
        jnp.float32
    )
    attended = lax.psum(rounded_partial.astype(jnp.bfloat16), "tp").astype(jnp.float32)
    mixed = residual.astype(jnp.float32) + attended
    normal_rows = rms_scale(mixed, mix_gain).astype(jnp.bfloat16)
    group_count = router_group.shape[1]
    expert_count = router_expert.shape[1]
    group_prob = jax.nn.softmax(
        jnp.dot(normal_rows, router_group, preferred_element_type=jnp.float32), axis=-1
    )
    logits = jnp.dot(normal_rows, router_expert, preferred_element_type=jnp.float32)
    chosen_group = expert_ids[:, 0] // (expert_count // group_count)
    group_pick = jnp.sum(
        jnp.where(chosen_group[:, None] == jnp.arange(group_count)[None, :], group_prob, 0.0),
        axis=1,
    )
    expert_match = expert_ids[:, :, None] == jnp.arange(expert_count)[None, None, :]
    chosen_logits = jnp.sum(jnp.where(expert_match, logits[:, None, :], 0.0), axis=2)
    gates = group_pick[:, None] * jax.nn.softmax(chosen_logits, axis=-1)
    tp_size = lax.axis_size("tp")
    sp_size = lax.axis_size("sp")
    capacity = tp_size * max(1, 4 * tok_rows // (expert_count * tp_size))
    flat_ids = expert_ids.reshape(-1)
    one_hot = (flat_ids[:, None] == jnp.arange(expert_count)[None, :]).astype(jnp.int32)
    earlier = jnp.cumsum(one_hot, axis=0) - one_hot
    slot_index = jnp.sum(earlier * one_hot, axis=1)
    target = flat_ids * capacity + slot_index
    source_row = jnp.arange(flat_ids.shape[0], dtype=jnp.int32) // 2
    row_of_slot = jnp.zeros((expert_count * capacity,), jnp.int32).at[target].set(source_row)
    slot_used = jnp.zeros((expert_count * capacity,), jnp.bool_).at[target].set(True)
    outgoing = jnp.where(slot_used[:, None], normal_rows[row_of_slot], jnp.zeros((), jnp.bfloat16))
    outgoing = outgoing.reshape(expert_count, capacity, -1)
    expert_rows = lax.all_to_all(outgoing, "sp", split_axis=0, concat_axis=1, tiled=True)
    lead_blocks = 1
    gate_part = jnp.einsum(
        "erd,edf->erf", expert_rows, expert_gate_w, preferred_element_type=jnp.float32
    )
    up_part = jnp.einsum(
        "erd,edf->erf", expert_rows, expert_up_w, preferred_element_type=jnp.float32
    )
    hidden = (jax.nn.silu(gate_part) * up_part).astype(jnp.bfloat16)
    down_part = jnp.einsum(
        "erf,efd->erd", hidden, expert_down_w, preferred_element_type=jnp.float32
    )
    rounded_down = lax.optimization_barrier(down_part.astype(jnp.bfloat16)).astype(jnp.float32)
    expert_out = lax.psum_scatter(
        rounded_down.astype(jnp.bfloat16), "tp", scatter_dimension=2, tiled=True
    )
    column_count = expert_out.shape[2]
    shaped_out = expert_out.reshape(expert_out.shape[0], lead_blocks, sp_size, -1, column_count)
    returned = lax.all_to_all(shaped_out, "sp", split_axis=2, concat_axis=0, tiled=True)
    returned = returned.reshape(expert_count * capacity, column_count)
    picked = returned[target].astype(jnp.float32).reshape(tok_rows, 2, column_count)
    combined = jnp.sum(picked * gates[:, :, None], axis=1)
    own_columns = lax.dynamic_slice_in_dim(
        mixed, lax.axis_index("tp") * column_count, column_count, 1
    )
    return (own_columns + combined).astype(jnp.bfloat16)


def solution(mesh):
    placed = (
        P("sp", None),
        P("sp", None),
        P("sp", None),
        P(),
        P("sp", "tp"),
        P("sp", "tp"),
        P(None, "tp"),
        P(None, "tp"),
        P(None, "tp"),
        P(None, "tp"),
        P("tp", None),
        P("tp", None),
        P(),
        P(),
        P(),
        P("sp", None),
        P("sp", None, "tp"),
        P("sp", None, "tp"),
        P("sp", "tp", None),
    )
    return jax.shard_map(
        shards, mesh=mesh, in_specs=placed, out_specs=P("sp", "tp"), check_vma=False
    )
```

profile of v0, /device:TPU:0, one launch (start us, length us, event | category | flops | bytes accessed | tf_op | source)
XLA Modules:
  0.0 230.2 jit_solution(13567661316674832507)
XLA Ops:
  6.6 0.9 convert_element_type.96
  7.5 1.1 copy.55
  8.6 1.0 copy.69
  9.8 15.7 %all-gather = bf16[8,112,64]{1,2,0:T(8,128)(2,1)S(1)} all-gather(bf16[1,112,64]{1,2,0:T(8,128)(2,1)S(1)} %maximum_bitcast_fusion), channel_id=1, replica_groups=mesh['sp'=8,'tp'=4] {'sp'}, dimensions={0}, use_global_device_ids=true | all-gather | bytes 129024 | tf_op jit(solution)/shard_map/all_gather | solution.py:129
  25.7 1.0 fusion.36
  26.8 1.0 fusion.38
  27.8 16.2 %all_gather.6 = bf16[896,512]{1,0:T(8,128)(2,1)S(1)} all-gather(bf16[112,512]{1,0:T(8,128)(2,1)S(1)} %fusion.38), channel_id=1, replica_groups=mesh['sp'=8,'tp'=4] {'sp'}, dimensions={0}, use_global_device_ids=true | all-gather | bytes 1032192 | tf_op jit(solution)/shard_map/all_gather | solution.py:123
  47.1 0.9 select_reduce_fusion
  52.5 1.1 fusion.12
  55.2 1.3 scatter_custom_fusion.1
  56.5 1.4 scatter_custom_fusion
  58.0 42.1 %all-reduce.3.cloned.1.call-done = bf16[112,2048]{1,0:T(8,128)(2,1)} async-done(((bf16[112,2048]{1,0:T(8,128)(2,1)}), bf16[112,2048]{1,0:T(8,128)(2,1)}) %all-reduce.3.cloned.1.call-update) | async-done | bytes 458768 | tf_op jit(solution)/shard_map/psum | solution.py:149
  100.2 2.3 convert_add_fusion
  102.7 3.2 %gather_fusion = bf16[448,2048]{1,0:T(8,128)(2,1)} fusion(bf16[112,2048]{1,0:T(8,128)(2,1)S(1)} %multiply_convert_fusion.1, s32[1024]{0:T(1024)S(1)} %pad_clamp_fusion.1), kind=kCustom, calls=%fused_computation | custom fusion | bytes 3671808 | tf_op jit(solution)/shard_map/gather | solution.py:177
  105.9 1.8 broadcast_select_fusion
  107.8 47.8 %all_to_all.8 = bf16[8,56,2048]{2,1,0:T(8,128)(2,1)S(1)} all-to-all(bf16[8,56,2048]{2,1,0:T(8,128)(2,1)S(1)} %broadcast_select_fusion), channel_id=1, replica_groups=mesh['sp'=8,'tp'=4] {'sp'}, dimensions={0} | all-to-all | bytes 3670016 | tf_op jit(solution)/shard_map/all_to_all | solution.py:179
  155.6 1.3 copy-done.1
  156.8 3.3 %fusion.4 = f32[448,1024]{1,0:T(8,128)} fusion(bf16[448,2048]{1,0:T(8,128)(2,1)S(1)} %bitcast.98, bf16[1,2048,1024]{2,1,0:T(8,128)(2,1)S(1)} %copy-done.11), kind=kOutput, calls=%fused_computation.8 | convolution fusion | flops 1879048192 | bytes 7864320 | tf_op jit(solution)/shard_map/erd,edf->erf/dot_general | solution.py:181
  160.2 9.8 %fusion.9 = bf16[1,448,2048]{2,1,0:T(8,128)(2,1)} fusion(bf16[1,1024,2048]{2,1,0:T(8,128)(2,1)} %param.37, f32[448,1024]{1,0:T(8,128)} %fusion.4, bf16[448,2048]{1,0:T(8,128)(2,1)} %bitcast.99, bf16[1,2048,1024]{2,1,0:T(8,128)(2,1)} %param.36), kind=kOutput, calls=%fused_computation.11 | convolution fusion | flops 3761766400 | bytes 13893632 | tf_op jit(solution)/shard_map/erf,efd->erd/dot_general | solution.py:188
  171.0 30.2 %reduce-scatter.2.cloned.1.call-done = bf16[1,448,512]{2,1,0:T(8,128)(2,1)} async-done(((bf16[1,448,2048]{2,1,0:T(8,128)(2,1)}), bf16[1,448,512]{2,1,0:T(8,128)(2,1)}) %reduce-scatter.2.cloned.1.call-update) | async-done | bytes 458768 | tf_op jit(solution)/shard_map/reduce_scatter | solution.py:192
  201.2 4.6 %all-to-all-start.1 = ((bf16[1,1,8,56,512]{4,3,1,0,2:T(8,128)(2,1)}), bf16[1,1,8,56,512]{4,3,1,0,2:T(8,128)(2,1)S(1)}, u32[]{:S(2)}, u32[]{:S(2)}) async-start(bf16[1,1,8,56,512]{4,3,1,0,2:T(8,128)(2,1)} %bitcast.106), calls=%async_computation.2 | async-start | bytes 917504 | tf_op jit(solution)/shard_map/all_to_all | solution.py:197
  206.3 13.4 %all-to-all-done.1 = bf16[1,1,8,56,512]{4,3,1,0,2:T(8,128)(2,1)S(1)} async-done(((bf16[1,1,8,56,512]{4,3,1,0,2:T(8,128)(2,1)}), bf16[1,1,8,56,512]{4,3,1,0,2:T(8,128)(2,1)S(1)}, u32[]{:S(2)}, u32[]{:S(2)}) %all-to-all-start.1) | async-done | bytes 458784 | tf_op jit(solution)/shard_map/all_to_all | solution.py:197
  219.7 1.1 gather_fusion.1
  221.7 1.6 add_convert_fusion
  (89 shorter events, 12.1 us)
Async XLA Ops:
  6.5 44.7 %copy-start = (bf16[512,2048]{1,0:T(8,128)(2,1)S(1)}, bf16[512,2048]{1,0:T(8,128)(2,1)}, u32[]{:S(2)}) copy-start(bf16[512,2048]{1,0:T(8,128)(2,1)} %param.29) | copy-start | bytes 6291460
  6.5 37.5 %copy-start.12 = (bf16[512,512]{1,0:T(8,128)(2,1)S(1)}, bf16[512,512]{1,0:T(8,128)(2,1)}, u32[]{:S(2)}) copy-start(bf16[512,512]{1,0:T(8,128)(2,1)} %param.25) | copy-start | bytes 1572868
  6.5 93.6 %all-reduce.3.cloned.1.call-start = ((), (), s32[]{:S(2)}) async-start(), calls=%async_computation.3 | async-start | bytes 917504 | tf_op jit(solution)/shard_map/psum | solution.py:149
  44.8 1.0 copy-start.5
  47.1 1.0 copy-start.6
  47.1 1.4 copy-start.13
  51.3 1.2 copy-start.4
  51.8 1.9 copy-start.9
  51.8 48.4 %copy-start.2 = (bf16[112,2048]{1,0:T(8,128)(2,1)S(1)}, bf16[112,2048]{1,0:T(8,128)(2,1)}, u32[]{:S(2)}) copy-start(bf16[112,2048]{1,0:T(8,128)(2,1)} %param.19) | copy-start | bytes 1376260
  53.6 48.8 %copy-start.10 = (f32[2048]{0:T(1024)S(1)}, f32[2048]{0:T(1024)}, u32[]{:S(2)}) copy-start(f32[2048]{0:T(1024)} %param.31) | copy-start | bytes 24580
  53.7 147.5 %reduce-scatter.2.cloned.1.call-start = ((), (), s32[]{:S(2)}) async-start(), calls=%async_computation.4 | async-start | bytes 2293760 | tf_op jit(solution)/shard_map/reduce_scatter | solution.py:192
  100.2 2.3 %copy-start.3 = (bf16[112,2048]{1,0:T(8,128)(2,1)S(1)}, bf16[112,2048]{1,0:T(8,128)(2,1)}, u32[]{:S(2)}) copy-start(bf16[112,2048]{1,0:T(8,128)(2,1)} %all-reduce.3.cloned.1.call-done) | copy-start | bytes 1376260
  105.9 50.9 %copy-start.11 = (bf16[1,2048,1024]{2,1,0:T(8,128)(2,1)S(1)}, bf16[1,2048,1024]{2,1,0:T(8,128)(2,1)}, u32[]{:S(2)}) copy-start(bf16[1,2048,1024]{2,1,0:T(8,128)(2,1)} %param.35) | copy-start | bytes 12582916
  155.6 1.3 copy-start.1
  170.0 0.8 copy-start.7
  170.0 35.8 %copy-start.8 = (bf16[2048,4]{0,1:T(4,128)(2,1)S(1)}, bf16[2048,4]{0,1:T(4,128)(2,1)}, u32[]{:S(2)}) copy-start(bf16[2048,4]{0,1:T(4,128)(2,1)} %param.32) | copy-start | bytes 49156
  201.2 18.5 %all-to-all-start.1 = ((bf16[1,1,8,56,512]{4,3,1,0,2:T(8,128)(2,1)}), bf16[1,1,8,56,512]{4,3,1,0,2:T(8,128)(2,1)S(1)}, u32[]{:S(2)}, u32[]{:S(2)}) async-start(bf16[1,1,8,56,512]{4,3,1,0,2:T(8,128)(2,1)} %bitcast.106), calls=%async_computation.2 | async-start | bytes 917504 | tf_op jit(solution)/shard_map/all_to_all | solution.py:197
Sparse Core Ops, SparseCore 0:
  53.8 46.3 all-reduce.2
  170.2 30.9 reduce-scatter.1
where the time goes:
time: 231 us; the launch traced here: 230 us
  waiting for transfers between devices  85.8 us (37%)
  blocking collectives  79.8 us (35%)
  matrix products  20.9 us (9%)
  between operations  13.8 us (6%)
  local copies, waits for them, and re-layouts  13.7 us (6%)
  other arithmetic  11.6 us (5%)
  starting transfers between devices  4.66 us (2%)
    all_to_all x1, blocking collectives, shards(): lax.all_to_all(outgoing, 'sp', split_axis=0, concat_axis=1, tiled=True)  47.8 us
    psum x1, waiting for transfers between devices, shards(): lax.psum(rounded_partial.astype(jnp.bfloat16), 'tp').astype(jnp.float32)  42.1 us
    reduce_scatter x1, waiting for transfers between devices, shards(): lax.psum_scatter(rounded_down.astype(jnp.bfloat16), 'tp', scatter_dimensi...  30.2 us
    all_gather x1, blocking collectives, shards(): lax.all_gather(normed, 'sp', axis=0, tiled=True)  16.2 us
    all_gather x1, blocking collectives, shards(): key_rot = lax.all_gather(key_turned, 'sp', axis=0, tiled=True)  15.7 us
    all_to_all x1, waiting for transfers between devices, shards(): lax.all_to_all(shaped_out, 'sp', split_axis=2, concat_axis=0, tiled=True)  13.4 us
    dot_general x1, matrix products, shards(): jnp.einsum('erf,efd->erd', hidden, expert_down_w, preferred_element_type=...  9.82 us
  transfers between devices with their start and end apart: 3, of which 3 were waited for; matrix products, arithmetic and copies ran while one was open for 2% of the time, Pallas kernels for 0%

commit v1 on v0

--- a/solution.py
+++ b/solution.py
@@ -2,6 +2,7 @@
 import jax.numpy as jnp
 from jax import lax
 from jax.sharding import PartitionSpec as P
+from jax.lax import all_gather
 
 PLAIN_KEY_WIDTH = 128
 LARGE_VALUE_SIZE = 128
@@ -100,6 +101,11 @@
     expert_up_w,
     expert_down_w,
 ):
+
+    def try_all_column_by_axis(frame_in):
+        q_next = jnp.sum(all_gather(frame_in, "tp"), 0)
+        return q_next
+
     tok_rows = latent.shape[0]
     positions = lax.axis_index("sp") * tok_rows + jnp.arange(tok_rows, dtype=jnp.int32)
     angles = angle_table(positions, ROPE)
@@ -146,7 +152,7 @@
     rounded_partial = lax.optimization_barrier(partial_value.astype(jnp.bfloat16)).astype(
         jnp.float32
     )
-    attended = lax.psum(rounded_partial.astype(jnp.bfloat16), "tp").astype(jnp.float32)
+    attended = try_all_column_by_axis(rounded_partial.astype(jnp.bfloat16)).astype(jnp.float32)
     mixed = residual.astype(jnp.float32) + attended
     normal_rows = rms_scale(mixed, mix_gain).astype(jnp.bfloat16)
     group_count = router_group.shape[1]

time: 231 us -> 220 us (0.952)
  waiting for transfers between devices: 85.8 us -> 73.9 us
    psum x1 -> x0, waiting for transfers between devices: 42.1 us -> none  [shards(): lax.psum(rounded_partial.astype(jnp.bfloat16), 'tp').astype(jnp.float32)]
    all_gather x0 -> x1, waiting for transfers between devices: none -> 30.3 us  [try_all_column_by_axis(): q_next = jnp.sum(all_gather(frame_in, 'tp'), 0)]
where the time goes in v1:
time: 220 us; the launch traced here: 219 us
  blocking collectives  79.8 us (36%)
  waiting for transfers between devices  73.9 us (34%)
  matrix products  20.9 us (10%)
  local copies, waits for them, and re-layouts  13.9 us (6%)
  between operations  13.8 us (6%)
  other arithmetic  12.4 us (6%)
  starting transfers between devices  4.65 us (2%)
    all_to_all x1, blocking collectives, shards(): lax.all_to_all(outgoing, 'sp', split_axis=0, concat_axis=1, tiled=True)  47.8 us
    all_gather x1, waiting for transfers between devices, try_all_column_by_axis(): q_next = jnp.sum(all_gather(frame_in, 'tp'), 0)  30.3 us
    reduce_scatter x1, waiting for transfers between devices, shards(): lax.psum_scatter(rounded_down.astype(jnp.bfloat16), 'tp', scatter_dimensi...  30.2 us
    all_gather x1, blocking collectives, shards(): lax.all_gather(normed, 'sp', axis=0, tiled=True)  16.2 us
    all_gather x1, blocking collectives, shards(): key_rot = lax.all_gather(key_turned, 'sp', axis=0, tiled=True)  15.7 us
    all_to_all x1, waiting for transfers between devices, shards(): lax.all_to_all(shaped_out, 'sp', split_axis=2, concat_axis=0, tiled=True)  13.4 us
    dot_general x1, matrix products, shards(): jnp.einsum('erf,efd->erd', hidden, expert_down_w, preferred_element_type=...  9.82 us
    all_to_all x1, starting transfers between devices, shards(): lax.all_to_all(shaped_out, 'sp', split_axis=2, concat_axis=0, tiled=True)  4.61 us
  transfers between devices with their start and end apart: 3, of which 3 were waited for; matrix products, arithmetic and copies ran while one was open for 2% of the time, Pallas kernels for 0%

profile of v1, /device:TPU:0, one launch (start us, length us, event | category | flops | bytes accessed | tf_op | source)
XLA Modules:
  0.0 219.2 jit_solution(10030827468064611122)
XLA Ops:
  6.6 0.9 convert_element_type.98
  7.5 1.1 copy.55
  8.6 1.0 copy.69
  9.8 15.7 %all-gather.1 = bf16[8,112,64]{1,2,0:T(8,128)(2,1)S(1)} all-gather(bf16[1,112,64]{1,2,0:T(8,128)(2,1)S(1)} %maximum_bitcast_fusion), channel_id=1, replica_groups=mesh['sp'=8,'tp'=4] {'sp'}, dimensions={0}, use_global_device_ids=true | all-gather | bytes 129024 | tf_op jit(solution)/shard_map/all_gather | solution.py:135
  25.7 1.0 fusion.36
  26.8 1.0 fusion.38
  27.8 16.2 %all_gather.12 = bf16[896,512]{1,0:T(8,128)(2,1)S(1)} all-gather(bf16[112,512]{1,0:T(8,128)(2,1)S(1)} %fusion.38), channel_id=1, replica_groups=mesh['sp'=8,'tp'=4] {'sp'}, dimensions={0}, use_global_device_ids=true | all-gather | bytes 1032192 | tf_op jit(solution)/shard_map/all_gather | solution.py:129
  52.5 1.1 fusion.12
  55.2 1.3 scatter_custom_fusion.1
  56.5 1.5 scatter_custom_fusion
  58.2 30.3 %all-gather.4.cloned.1.call-done = bf16[448,2048]{1,0:T(8,128)(2,1)} async-done(((bf16[112,2048]{1,0:T(8,128)(2,1)}), bf16[448,2048]{1,0:T(8,128)(2,1)}) %all-gather.4.cloned.1.call-update) | async-done | bytes 1835024 | tf_op jit(solution)/shard_map/all_gather | solution.py:106
  88.5 1.9 reduce_sum.107
  90.3 1.2 convert_add_fusion
  91.8 3.2 %gather_fusion = bf16[448,2048]{1,0:T(8,128)(2,1)} fusion(bf16[112,2048]{1,0:T(8,128)(2,1)S(1)} %multiply_convert_fusion.1, s32[1024]{0:T(1024)S(1)} %pad_clamp_fusion.1), kind=kCustom, calls=%fused_computation | custom fusion | bytes 3671808 | tf_op jit(solution)/shard_map/gather | solution.py:183
  95.0 1.8 broadcast_select_fusion
  96.8 47.8 %all_to_all.8 = bf16[8,56,2048]{2,1,0:T(8,128)(2,1)S(1)} all-to-all(bf16[8,56,2048]{2,1,0:T(8,128)(2,1)S(1)} %broadcast_select_fusion), channel_id=1, replica_groups=mesh['sp'=8,'tp'=4] {'sp'}, dimensions={0} | all-to-all | bytes 3670016 | tf_op jit(solution)/shard_map/all_to_all | solution.py:185
  144.7 1.3 copy-done.1
  145.9 3.3 %fusion.4 = f32[448,1024]{1,0:T(8,128)} fusion(bf16[448,2048]{1,0:T(8,128)(2,1)S(1)} %bitcast.100, bf16[1,2048,1024]{2,1,0:T(8,128)(2,1)S(1)} %copy-done.10), kind=kOutput, calls=%fused_computation.8 | convolution fusion | flops 1879048192 | bytes 7864320 | tf_op jit(solution)/shard_map/erd,edf->erf/dot_general | solution.py:187
  149.3 9.8 %fusion.9 = bf16[1,448,2048]{2,1,0:T(8,128)(2,1)} fusion(bf16[1,1024,2048]{2,1,0:T(8,128)(2,1)} %param.37, f32[448,1024]{1,0:T(8,128)} %fusion.4, bf16[448,2048]{1,0:T(8,128)(2,1)} %bitcast.101, bf16[1,2048,1024]{2,1,0:T(8,128)(2,1)} %param.36), kind=kOutput, calls=%fused_computation.11 | convolution fusion | flops 3761766400 | bytes 13893632 | tf_op jit(solution)/shard_map/erf,efd->erd/dot_general | solution.py:194
  160.1 30.2 %reduce-scatter.2.cloned.1.call-done = bf16[1,448,512]{2,1,0:T(8,128)(2,1)} async-done(((bf16[1,448,2048]{2,1,0:T(8,128)(2,1)}), bf16[1,448,512]{2,1,0:T(8,128)(2,1)}) %reduce-scatter.2.cloned.1.call-update) | async-done | bytes 458768 | tf_op jit(solution)/shard_map/reduce_scatter | solution.py:198
  190.2 4.6 %all-to-all-start.1 = ((bf16[1,1,8,56,512]{4,3,1,0,2:T(8,128)(2,1)}), bf16[1,1,8,56,512]{4,3,1,0,2:T(8,128)(2,1)S(1)}, u32[]{:S(2)}, u32[]{:S(2)}) async-start(bf16[1,1,8,56,512]{4,3,1,0,2:T(8,128)(2,1)} %bitcast.108), calls=%async_computation.2 | async-start | bytes 917504 | tf_op jit(solution)/shard_map/all_to_all | solution.py:203
  195.4 13.4 %all-to-all-done.1 = bf16[1,1,8,56,512]{4,3,1,0,2:T(8,128)(2,1)S(1)} async-done(((bf16[1,1,8,56,512]{4,3,1,0,2:T(8,128)(2,1)}), bf16[1,1,8,56,512]{4,3,1,0,2:T(8,128)(2,1)S(1)}, u32[]{:S(2)}, u32[]{:S(2)}) %all-to-all-start.1) | async-done | bytes 458784 | tf_op jit(solution)/shard_map/all_to_all | solution.py:203
  208.8 1.1 gather_fusion.1
  210.8 1.6 add_convert_fusion
  (88 shorter events, 13.0 us)
Async XLA Ops:
  6.5 44.8 %copy-start = (bf16[512,2048]{1,0:T(8,128)(2,1)S(1)}, bf16[512,2048]{1,0:T(8,128)(2,1)}, u32[]{:S(2)}) copy-start(bf16[512,2048]{1,0:T(8,128)(2,1)} %param.29) | copy-start | bytes 6291460
  6.5 37.5 %copy-start.11 = (bf16[512,512]{1,0:T(8,128)(2,1)S(1)}, bf16[512,512]{1,0:T(8,128)(2,1)}, u32[]{:S(2)}) copy-start(bf16[512,512]{1,0:T(8,128)(2,1)} %param.25) | copy-start | bytes 1572868
  6.5 81.9 %all-gather.4.cloned.1.call-start = ((), (), s32[]{:S(2)}) async-start(), calls=%async_computation.4 | async-start | bytes 2293760 | tf_op jit(solution)/shard_map/all_gather | solution.py:106
  44.8 1.0 copy-start.4
  47.1 1.0 copy-start.5
  47.1 1.4 copy-start.12
  51.3 1.2 copy-start.3
  51.8 1.9 copy-start.8
  53.6 36.7 %copy-start.2 = (bf16[112,2048]{1,0:T(8,128)(2,1)S(1)}, bf16[112,2048]{1,0:T(8,128)(2,1)}, u32[]{:S(2)}) copy-start(bf16[112,2048]{1,0:T(8,128)(2,1)} %param.19) | copy-start | bytes 1376260
  53.7 136.6 %reduce-scatter.2.cloned.1.call-start = ((), (), s32[]{:S(2)}) async-start(), calls=%async_computation.3 | async-start | bytes 2293760 | tf_op jit(solution)/shard_map/reduce_scatter | solution.py:198
  88.5 3.1 %copy-start.9 = (f32[2048]{0:T(1024)S(1)}, f32[2048]{0:T(1024)}, u32[]{:S(2)}) copy-start(f32[2048]{0:T(1024)} %param.31) | copy-start | bytes 24580
  95.0 50.9 %copy-start.10 = (bf16[1,2048,1024]{2,1,0:T(8,128)(2,1)S(1)}, bf16[1,2048,1024]{2,1,0:T(8,128)(2,1)}, u32[]{:S(2)}) copy-start(bf16[1,2048,1024]{2,1,0:T(8,128)(2,1)} %param.35) | copy-start | bytes 12582916
  144.7 1.3 copy-start.1
  159.1 0.8 copy-start.6
  159.1 35.8 %copy-start.7 = (bf16[2048,4]{0,1:T(4,128)(2,1)S(1)}, bf16[2048,4]{0,1:T(4,128)(2,1)}, u32[]{:S(2)}) copy-start(bf16[2048,4]{0,1:T(4,128)(2,1)} %param.32) | copy-start | bytes 49156
  190.2 18.5 %all-to-all-start.1 = ((bf16[1,1,8,56,512]{4,3,1,0,2:T(8,128)(2,1)}), bf16[1,1,8,56,512]{4,3,1,0,2:T(8,128)(2,1)S(1)}, u32[]{:S(2)}, u32[]{:S(2)}) async-start(bf16[1,1,8,56,512]{4,3,1,0,2:T(8,128)(2,1)} %bitcast.108), calls=%async_computation.2 | async-start | bytes 917504 | tf_op jit(solution)/shard_map/all_to_all | solution.py:203
Sparse Core Ops, SparseCore 0:
  53.8 34.6 all-gather.3
  159.2 30.9 reduce-scatter.1
